TPU v7x, 32 devices: a whole 2x2x4 slice. The times are simulated.
32 devices in a mesh: sp: 8 (over z, x), tp: 4 (over y, core).
Axes of the slice: x: 2, y: 2, z: 4, core: 2. Of those that a mesh axis runs over, the one named last changes fastest.
Arguments:
- out_grad: bfloat16 [1024, 2048], P('sp', 'tp'), may hold values from -6 to 6
- moe_input: bfloat16 [1024, 2048], P('sp', 'tp'), may hold values from -6 to 6
- route_weight: float32 [1024, 2], P('sp'), may hold values from 0.2 to 1
- route_ids: int32 [1024, 2], P('sp'), may hold values from 0 to 7, all different within a row; in each aligned block of 128 rows (0 to 127, 128 to 255, ...) at most 64 rows name the same one
- gate_proj: bfloat16 [8, 2048, 2816], P('sp', None, 'tp'), may hold values from -0.125 to 0.125
- up_proj: bfloat16 [8, 2048, 2816], P('sp', None, 'tp'), may hold values from -0.125 to 0.125
- down_proj: bfloat16 [8, 2816, 2048], P('sp', 'tp'), may hold values from -0.109375 to 0.109375
- out_proj: bfloat16 [2048, 2048], P(None, 'tp'), may hold values from -0.125 to 0.125
- conv_out: bfloat16 [1024, 2048], P('sp', 'tp'), may hold values from -6 to 6
- gate_b: bfloat16 [1024, 2048], P('sp', 'tp'), may hold values from -6 to 6
- gate_c: bfloat16 [1024, 2048], P('sp', 'tp'), may hold values from -6 to 6
- value_v: bfloat16 [1024, 2048], P('sp', 'tp'), may hold values from -6 to 6
- conv_taps: float32 [3, 2048], P(None, 'tp'), may hold values from -3 to 3
Outputs:
- grad_gate: bfloat16 [8, 2048, 2816], P('sp', None, 'tp')
- grad_up: bfloat16 [8, 2048, 2816], P('sp', None, 'tp')
- grad_down: bfloat16 [8, 2816, 2048], P('sp', 'tp')
- grad_out: float32 [2048, 2048], P('sp', 'tp')
- grad_b: bfloat16 [1024, 2048], P('sp', 'tp')
- grad_c: bfloat16 [1024, 2048], P('sp', 'tp')
- grad_v: bfloat16 [1024, 2048], P('sp', 'tp')
Inputs may be any that keep to these rules, and one draw needn't show every extreme that they name: `route_ids`: each row names two different experts; within the 128 rows of one index of sp no expert is named by more than 64 rows, a bound that some block reaches.
All inputs are finite; a program needn't handle non-finite values.
Results may differ from a plain program's by a relative error of at most 0.019.
Values may be sent and summed in bfloat16 or wider, within the bound.
A program may use at most 64 MiB of HBM per device.

v0:
```python
import jax
import jax.numpy as jnp
from jax import lax
from jax.sharding import PartitionSpec as P


def with_halo(block, sides, width):
    for axis, dim in sides:
        count = lax.axis_size(axis)
        forward = [(i, i + 1) for i in range(count - 1)]
        backward = [(target, source) for source, target in forward]
        low = lax.ppermute(
            lax.slice_in_dim(block, block.shape[dim] - width, None, axis=dim), axis, forward
        )
        high = lax.ppermute(lax.slice_in_dim(block, 0, width, axis=dim), axis, backward)
        block = jnp.concatenate([low, block, high], axis=dim)
    return block


def place_rows(rows, index, total):
    return jnp.zeros((total, rows.shape[1]), rows.dtype).at[index].set(rows)


def local(
    out_grad,
    moe_input,
    route_weight,
    route_ids,
    gate_proj,
    up_proj,
    down_proj,
    out_proj,
    conv_out,
    gate_b,
    gate_c,
    value_v,
    conv_taps,
):
    tok_rows = out_grad.shape[0]
    local_cols = out_grad.shape[1]
    n_experts = lax.axis_size("sp")
    capacity = 4 * tok_rows // n_experts
    flat = route_ids.reshape(2 * tok_rows)
    onehot = (flat[:, None] == jnp.arange(n_experts, dtype=jnp.int32)[None, :]).astype(jnp.int32)
    before = jnp.cumsum(onehot, axis=0) - onehot
    slot = jnp.sum(before * onehot, axis=1)
    dest = flat * capacity + slot
    total = n_experts * capacity
    rows_x = jnp.broadcast_to(moe_input[:, None, :], (tok_rows, 2, local_cols)).reshape(
        2 * tok_rows, local_cols
    )
    rows_dy = (
        (route_weight[:, :, None] * out_grad.astype(jnp.float32)[:, None, :])
        .astype(jnp.bfloat16)
        .reshape(2 * tok_rows, local_cols)
    )
    send_x = place_rows(rows_x, dest, total).reshape(n_experts, capacity, local_cols)
    send_dy = place_rows(rows_dy, dest, total).reshape(n_experts, capacity, local_cols)
    part_x, part_dy = (
        lax.all_to_all(send_x, "sp", split_axis=0, concat_axis=0, tiled=True),
        lax.all_to_all(send_dy, "sp", split_axis=0, concat_axis=0, tiled=True),
    )
    recv_x, recv_dy = (
        lax.all_gather(part_x, "tp", axis=2, tiled=True),
        lax.all_gather(part_dy, "tp", axis=2, tiled=True),
    )
    width = recv_x.shape[2]
    xin = recv_x.reshape(total, width)
    dyin = recv_dy.reshape(total, width)
    w_gate = gate_proj[0]
    w_up = up_proj[0]
    w_down = down_proj[0]
    gate = jnp.dot(xin, w_gate, preferred_element_type=jnp.float32)
    upval = jnp.dot(xin, w_up, preferred_element_type=jnp.float32)
    sig = jax.nn.sigmoid(gate)
    act = gate * sig
    hidden = (act * upval).astype(jnp.bfloat16)
    grad_down = jnp.dot(hidden.T, dyin, preferred_element_type=jnp.float32).astype(jnp.bfloat16)
    dhid = jnp.dot(dyin, w_down.T, preferred_element_type=jnp.float32)
    dgate = (dhid * upval * (sig * (1.0 + gate * (1.0 - sig)))).astype(jnp.bfloat16)
    dup = (dhid * act).astype(jnp.bfloat16)
    grad_gate = jnp.dot(xin.T, dgate, preferred_element_type=jnp.float32).astype(jnp.bfloat16)
    grad_up = jnp.dot(xin.T, dup, preferred_element_type=jnp.float32).astype(jnp.bfloat16)
    partial_value = jnp.dot(dgate, w_gate.T, preferred_element_type=jnp.float32) + jnp.dot(
        dup, w_up.T, preferred_element_type=jnp.float32
    )
    partial_value = lax.optimization_barrier(partial_value.astype(jnp.bfloat16)).astype(jnp.float32)
    summed = lax.psum_scatter(
        partial_value.astype(jnp.bfloat16), "tp", scatter_dimension=1, tiled=True
    )
    returned = lax.all_to_all(
        summed.reshape(n_experts, capacity, local_cols),
        "sp",
        split_axis=0,
        concat_axis=0,
        tiled=True,
    )
    picked = returned.reshape(total, local_cols)[dest]
    moe_grad = jnp.sum(picked.reshape(tok_rows, 2, local_cols).astype(jnp.float32), axis=1)
    grad_h = (out_grad.astype(jnp.float32) + moe_grad).astype(jnp.bfloat16)
    full_h = lax.all_gather(grad_h, "tp", axis=1, tiled=True)
    grad_z = jnp.dot(full_h, out_proj, preferred_element_type=jnp.float32)
    dconv = (grad_z * gate_b.astype(jnp.float32)).astype(jnp.bfloat16)
    grad_b = (grad_z * conv_out.astype(jnp.float32)).astype(jnp.bfloat16)
    padded = with_halo(dconv, (("sp", 0),), 1).astype(jnp.float32)
    grad_u = conv_taps[0] * padded[2:] + conv_taps[1] * padded[1:-1] + conv_taps[2] * padded[:-2]
    grad_c = (grad_u * value_v.astype(jnp.float32)).astype(jnp.bfloat16)
    grad_v = (grad_u * gate_c.astype(jnp.float32)).astype(jnp.bfloat16)
    mixed = (gate_b.astype(jnp.float32) * conv_out.astype(jnp.float32)).astype(jnp.bfloat16)
    grad_out = lax.psum_scatter(
        lax.dot_general(
            full_h, mixed, (((0,), (0,)), ((), ())), preferred_element_type=jnp.float32
        ).astype(jnp.bfloat16),
        "sp",
        scatter_dimension=0,
        tiled=True,
    ).astype(jnp.float32)
    return (grad_gate[None], grad_up[None], grad_down[None], grad_out, grad_b, grad_c, grad_v)


def solution(mesh):
    in_specs = (
        P("sp", "tp"),
        P("sp", "tp"),
        P("sp", None),
        P("sp", None),
        P("sp", None, "tp"),
        P("sp", None, "tp"),
        P("sp", "tp", None),
        P(None, "tp"),
        P("sp", "tp"),
        P("sp", "tp"),
        P("sp", "tp"),
        P("sp", "tp"),
        P(None, "tp"),
    )
    out_specs = (
        P("sp", None, "tp"),
        P("sp", None, "tp"),
        P("sp", "tp", None),
        P("sp", "tp"),
        P("sp", "tp"),
        P("sp", "tp"),
        P("sp", "tp"),
    )
    return jax.shard_map(local, mesh=mesh, in_specs=in_specs, out_specs=out_specs, check_vma=False)
```

profile of v0, /device:TPU:0, one launch (start us, length us, event | category | flops | bytes accessed | tf_op | source)
XLA Modules:
  0.0 235.2 jit_solution(585506620943027061)
XLA Ops:
  7.2 0.9 copy.21
  10.2 1.0 broadcast_in_dim.8
  11.3 0.8 reshape.112
  12.2 2.1 scatter_custom_fusion
  14.3 21.7 %all_to_all.15 = bf16[8,64,512]{2,1,0:T(8,128)(2,1)} all-to-all(bf16[8,64,512]{2,1,0:T(8,128)(2,1)S(1)} %bitcast.55), channel_id=1, replica_groups=mesh['sp'=8,'tp'=4] {'sp'}, dimensions={0} | all-to-all | bytes 1048576 | tf_op jit(solution)/shard_map/all_to_all | solution.py:60
  36.2 1.2 mul.110
  37.6 2.2 scatter_custom_fusion.1
  39.9 17.6 %all_to_all.16 = bf16[8,64,512]{2,1,0:T(8,128)(2,1)} all-to-all(bf16[8,64,512]{2,1,0:T(8,128)(2,1)S(1)} %bitcast.54), channel_id=1, replica_groups=mesh['sp'=8,'tp'=4] {'sp'}, dimensions={0} | all-to-all | bytes 1048576 | tf_op jit(solution)/shard_map/all_to_all | solution.py:61
  57.8 4.5 %fusion.5 = f32[512,704]{0,1:T(8,128)} fusion(bf16[512,2048]{1,0:T(8,128)(2,1)} %bitcast.64, bf16[1,2048,704]{1,2,0:T(8,128)(2,1)S(1)} %copy-done), kind=kOutput, calls=%fused_computation.13 | convolution fusion | flops 1476395008 | bytes 6422528 | tf_op jit(solution)/shard_map/dot_general | solution.py:73
  62.4 2.8 %fusion.8 = f32[512,704]{0,1:T(8,128)} fusion(bf16[512,2048]{1,0:T(8,128)(2,1)S(1)} %bitcast.66, bf16[1,2048,704]{1,2,0:T(8,128)(2,1)S(1)} %copy-done.11), kind=kOutput, calls=%fused_computation.16 | convolution fusion | flops 1476395008 | bytes 6422528 | tf_op jit(solution)/shard_map/dot_general | solution.py:74
  65.1 16.8 %all-gather.5.cloned.1.call-done = bf16[8,64,2048]{2,1,0:T(8,128)(2,1)} async-done(((bf16[8,64,512]{2,1,0:T(8,128)(2,1)}), bf16[8,64,2048]{2,1,0:T(8,128)(2,1)}) %all-gather.5.cloned.1.call-update) | async-done | bytes 2097168 | tf_op jit(solution)/shard_map/all_gather | solution.py:65
  81.9 5.4 %multiply_convert_fusion.1 = (bf16[512,704]{0,1:T(8,128)(2,1)S(1)}, bf16[512,704]{0,1:T(8,128)(2,1)S(1)}) fusion(f32[512,704]{0,1:T(8,128)} %fusion.5, f32[512,704]{0,1:T(8,128)} %fusion.8, bf16[512,2048]{1,0:T(8,128)(2,1)} %bitcast.68, bf16[1,704,2048]{2,1,0:T(8,128)(2,1)} %param.19), kind=kOutput, calls=%fused_computation.21 | convolution fusion | flops 1481080832 | bytes 9306112 | tf_op jit(solution)/shard_map/dot_general | solution.py:79
  87.3 1.9 fusion.3
  89.7 3.3 %add_convert_fusion = bf16[512,2048]{1,0:T(8,128)(2,1)} fusion(f32[512,2048]{1,0:T(8,128)S(1)} %fusion.3, bf16[512,704]{0,1:T(8,128)(2,1)S(1)} %get-tuple-element.9, bf16[1,2048,704]{1,2,0:T(8,128)(2,1)S(1)} %copy-done.12), kind=kOutput, calls=%fused_computation.3 | convolution fusion | flops 1478492160 | bytes 9895936 | tf_op jit(solution)/shard_map/dot_general | solution.py:84
  93.0 31.3 %reduce-scatter.3.cloned.1.call-done = bf16[512,512]{1,0:T(8,128)(2,1)} async-done(((bf16[512,2048]{1,0:T(8,128)(2,1)}), bf16[512,512]{1,0:T(8,128)(2,1)}) %reduce-scatter.3.cloned.1.call-update) | async-done | bytes 524304 | tf_op jit(solution)/shard_map/reduce_scatter | solution.py:88
  124.3 5.5 %all-to-all-start.2 = ((bf16[8,64,512]{2,1,0:T(8,128)(2,1)}), bf16[8,64,512]{2,1,0:T(8,128)(2,1)S(1)}, u32[]{:S(2)}, u32[]{:S(2)}) async-start(bf16[8,64,512]{2,1,0:T(8,128)(2,1)} %bitcast.56), calls=%async_computation.3 | async-start | bytes 1048576 | tf_op jit(solution)/shard_map/all_to_all | solution.py:91
  129.9 14.3 %all-to-all-done.2 = bf16[8,64,512]{2,1,0:T(8,128)(2,1)S(1)} async-done(((bf16[8,64,512]{2,1,0:T(8,128)(2,1)}), bf16[8,64,512]{2,1,0:T(8,128)(2,1)S(1)}, u32[]{:S(2)}, u32[]{:S(2)}) %all-to-all-start.2) | async-done | bytes 524320 | tf_op jit(solution)/shard_map/all_to_all | solution.py:91
  144.2 1.9 gather_fusion
  146.0 1.3 reshape.99
  147.3 1.3 reduce_sum.22
  148.7 1.0 add_convert_fusion.1
  149.7 6.7 %all_gather.11 = bf16[128,2048]{1,0:T(8,128)(2,1)S(1)} all-gather(bf16[128,512]{1,0:T(8,128)(2,1)S(1)} %add_convert_fusion.1), channel_id=1, replica_groups=mesh['sp'=8,'tp'=4] {'tp'}, dimensions={1}, use_global_device_ids=true | all-gather | bytes 655360 | tf_op jit(solution)/shard_map/all_gather | solution.py:101
  156.4 3.0 %convolution_convert_fusion.3 = bf16[2048,512]{1,0:T(8,128)(2,1)} fusion(bf16[128,2048]{1,0:T(8,128)(2,1)S(1)} %all_gather.11, bf16[128,512]{1,0:T(8,128)(2,1)S(1)} %copy-done.4, bf16[128,512]{1,0:T(8,128)(2,1)} %param.22), kind=kOutput, calls=%fused_computation.7 | convolution fusion | flops 269746176 | bytes 2883584 | tf_op jit(solution)/shard_map/dot_general | solution.py:111
  159.5 5.2 %fusion.2 = bf16[1,2048,704]{1,2,0:T(8,128)(2,1)} fusion(bf16[512,704]{0,1:T(8,128)(2,1)} %copy-done.16, bf16[512,2048]{1,0:T(8,128)(2,1)} %bitcast.65), kind=kOutput, calls=%fused_computation.10 | convolution fusion | flops 1477836800 | bytes 5701632 | tf_op jit(solution)/shard_map/dot_general | solution.py:83
  164.7 3.3 %fusion = bf16[1,704,2048]{2,1,0:T(8,128)(2,1)} fusion(bf16[512,2048]{1,0:T(8,128)(2,1)S(1)} %bitcast.69, f32[512,704]{0,1:T(8,128)S(1)} %copy-done.18, f32[512,704]{0,1:T(8,128)S(1)} %copy-done.17), kind=kOutput, calls=%fused_computation.8 | convolution fusion | flops 1479999488 | bytes 7864320 | tf_op jit(solution)/shard_map/dot_general | solution.py:78
  168.0 1.1 fusion.13
  169.2 3.4 %collective-permute-start = (bf16[1,512]{1,0:T(2,128)(2,1)S(1)}, bf16[1,512]{1,0:T(2,128)(2,1)S(1)}, u32[]{:S(2)}, u32[]{:S(2)}) collective-permute-start(bf16[1,512]{1,0:T(2,128)(2,1)S(1)} %get-tuple-element.13), channel_id=1, source_target_pairs={{0,4},{4,8},{8,12},{12,16},{16,20},{20,24},{24,28},{1,5},{5,9},{9,... | collective-permute-start | bytes 3080 | tf_op jit(solution)/shard_map/ppermute | solution.py:12
  172.6 1.4 collective-permute-start.1
  174.0 3.2 %fusion.1 = bf16[1,2048,704]{1,2,0:T(8,128)(2,1)} fusion(bf16[512,704]{0,1:T(8,128)(2,1)S(1)} %copy-done.3, bf16[512,2048]{1,0:T(8,128)(2,1)S(1)} %bitcast.67), kind=kOutput, calls=%fused_computation.9 | convolution fusion | flops 1477836800 | bytes 5701632 | tf_op jit(solution)/shard_map/dot_general | solution.py:82
  177.3 0.9 collective-permute-done.1
  179.7 47.1 %reduce-scatter.5.cloned.1.call-done = bf16[256,512]{1,0:T(8,128)(2,1)} async-done(((bf16[2048,512]{1,0:T(8,128)(2,1)}), bf16[256,512]{1,0:T(8,128)(2,1)}) %reduce-scatter.5.cloned.1.call-update) | async-done | bytes 262160 | tf_op jit(solution)/shard_map/reduce_scatter | solution.py:110
  226.8 1.8 convert_element_type.103
  (69 shorter events, 5.0 us)
Async XLA Ops:
  7.2 50.6 %copy-start = (bf16[1,2048,704]{1,2,0:T(8,128)(2,1)S(1)}, bf16[1,2048,704]{1,2,0:T(8,128)(2,1)}, u32[]{:S(2)}) copy-start(bf16[1,2048,704]{1,2,0:T(8,128)(2,1)} %param.17) | copy-start | bytes 8650756
  7.2 28.9 %copy-start.6 = (bf16[128,512]{1,0:T(8,128)(2,1)S(1)}, bf16[128,512]{1,0:T(8,128)(2,1)}, u32[]{:S(2)}) copy-start(bf16[128,512]{1,0:T(8,128)(2,1)} %param.13) | copy-start | bytes 393220
  7.2 50.6 %all-gather.3.cloned.1.call-start = ((), (), s32[]{:S(2)}) async-start(), calls=%async_computation.5 | async-start | bytes 2621440 | tf_op jit(solution)/shard_map/all_gather | solution.py:64
  11.3 26.1 %copy-start.10 = (f32[128,2]{0,1:T(2,128)S(1)}, f32[128,2]{0,1:T(2,128)}, u32[]{:S(2)}) copy-start(f32[128,2]{0,1:T(2,128)} %param.15) | copy-start | bytes 3076
  36.0 45.9 %all-gather.5.cloned.1.call-start = ((), (), s32[]{:S(2)}) async-start(), calls=%async_computation.6 | async-start | bytes 2621440 | tf_op jit(solution)/shard_map/all_gather | solution.py:65
  57.5 66.8 %reduce-scatter.3.cloned.1.call-start = ((), (), s32[]{:S(2)}) async-start(), calls=%async_computation.7 | async-start | bytes 2621440 | tf_op jit(solution)/shard_map/reduce_scatter | solution.py:88
  57.8 4.6 %copy-start.11 = (bf16[1,2048,704]{1,2,0:T(8,128)(2,1)S(1)}, bf16[1,2048,704]{1,2,0:T(8,128)(2,1)}, u32[]{:S(2)}) copy-start(bf16[1,2048,704]{1,2,0:T(8,128)(2,1)} %param.18) | copy-start | bytes 8650756
  57.8 4.5 %copy-start.13 = (bf16[8,64,2048]{2,1,0:T(8,128)(2,1)S(1)}, bf16[8,64,2048]{2,1,0:T(8,128)(2,1)}, u32[]{:S(2)}) copy-start(bf16[8,64,2048]{2,1,0:T(8,128)(2,1)} %all-gather.3.cloned.1.call-done) | copy-start | bytes 6291460
  87.3 1.9 copy-start.2
  87.3 1.9 copy-start.16
  87.3 2.3 copy-start.12
  124.3 19.8 %all-to-all-start.2 = ((bf16[8,64,512]{2,1,0:T(8,128)(2,1)}), bf16[8,64,512]{2,1,0:T(8,128)(2,1)S(1)}, u32[]{:S(2)}, u32[]{:S(2)}) async-start(bf16[8,64,512]{2,1,0:T(8,128)(2,1)} %bitcast.56), calls=%async_computation.3 | async-start | bytes 1048576 | tf_op jit(solution)/shard_map/all_to_all | solution.py:91
  129.9 97.0 %reduce-scatter.5.cloned.1.call-start = ((), (), s32[]{:S(2)}) async-start(), calls=%async_computation.8 | async-start | bytes 2359296 | tf_op jit(solution)/shard_map/reduce_scatter | solution.py:110
  144.2 12.2 %copy-start.4 = (bf16[128,512]{1,0:T(8,128)(2,1)S(1)}, bf16[128,512]{1,0:T(8,128)(2,1)}, u32[]{:S(2)}) copy-start(bf16[128,512]{1,0:T(8,128)(2,1)} %param.21) | copy-start | bytes 393220
  156.4 3.0 %copy-start.9 = (f32[3,512]{1,0:T(4,128)S(1)}, f32[3,512]{1,0:T(4,128)}, u32[]{:S(2)}) copy-start(f32[3,512]{1,0:T(4,128)} %param.25) | copy-start | bytes 18436
  159.5 5.2 %copy-start.15 = (bf16[8,64,2048]{2,1,0:T(8,128)(2,1)S(1)}, bf16[8,64,2048]{2,1,0:T(8,128)(2,1)}, u32[]{:S(2)}) copy-start(bf16[8,64,2048]{2,1,0:T(8,128)(2,1)} %all-gather.5.cloned.1.call-done) | copy-start | bytes 6291460
  159.5 5.2 %copy-start.17 = (f32[512,704]{0,1:T(8,128)S(1)}, f32[512,704]{0,1:T(8,128)}, u32[]{:S(2)}) copy-start(f32[512,704]{0,1:T(8,128)} %fusion.5) | copy-start | bytes 4325380
  159.5 5.2 %copy-start.18 = (f32[512,704]{0,1:T(8,128)S(1)}, f32[512,704]{0,1:T(8,128)}, u32[]{:S(2)}) copy-start(f32[512,704]{0,1:T(8,128)} %fusion.8) | copy-start | bytes 4325380
  164.7 3.3 %copy-start.1 = (bf16[2048,512]{1,0:T(8,128)(2,1)S(1)}, bf16[2048,512]{1,0:T(8,128)(2,1)}, u32[]{:S(2)}) copy-start(bf16[2048,512]{1,0:T(8,128)(2,1)} %param.20) | copy-start | bytes 6291460
  164.7 3.3 %copy-start.5 = (bf16[128,512]{1,0:T(8,128)(2,1)S(1)}, bf16[128,512]{1,0:T(8,128)(2,1)}, u32[]{:S(2)}) copy-start(bf16[128,512]{1,0:T(8,128)(2,1)} %param.22) | copy-start | bytes 393220
  168.0 6.0 %copy-start.3 = (bf16[512,704]{0,1:T(8,128)(2,1)S(1)}, bf16[512,704]{0,1:T(8,128)(2,1)}, u32[]{:S(2)}) copy-start(bf16[512,704]{0,1:T(8,128)(2,1)} %copy-done.2) | copy-start | bytes 2162692
  168.0 6.0 %copy-start.14 = (bf16[8,64,2048]{2,1,0:T(8,128)(2,1)S(1)}, bf16[8,64,2048]{2,1,0:T(8,128)(2,1)}, u32[]{:S(2)}) copy-start(bf16[8,64,2048]{2,1,0:T(8,128)(2,1)} %all-gather.3.cloned.1.call-done) | copy-start | bytes 6291460
  169.2 8.1 %collective-permute-start = (bf16[1,512]{1,0:T(2,128)(2,1)S(1)}, bf16[1,512]{1,0:T(2,128)(2,1)S(1)}, u32[]{:S(2)}, u32[]{:S(2)}) collective-permute-start(bf16[1,512]{1,0:T(2,128)(2,1)S(1)} %get-tuple-element.13), channel_id=1, source_target_pairs={{0,4},{4,8},{8,12},{12,16},{16,20},{20,24},{24,28},{1,5},{5,9},{9,... | collective-permute-start | bytes 3080 | tf_op jit(solution)/shard_map/ppermute | solution.py:12
  172.5 5.7 %copy-start.7 = (bf16[128,512]{1,0:T(8,128)(2,1)S(1)}, bf16[128,512]{1,0:T(8,128)(2,1)}, u32[]{:S(2)}) copy-start(bf16[128,512]{1,0:T(8,128)(2,1)} %param.23) | copy-start | bytes 393220
  172.6 6.4 %copy-start.8 = (bf16[128,512]{1,0:T(8,128)(2,1)S(1)}, bf16[128,512]{1,0:T(8,128)(2,1)}, u32[]{:S(2)}) copy-start(bf16[128,512]{1,0:T(8,128)(2,1)} %param.24) | copy-start | bytes 393220
  172.6 5.6 %collective-permute-start.1 = (bf16[1,512]{1,0:T(2,128)(2,1)S(1)}, bf16[1,512]{1,0:T(2,128)(2,1)S(1)}, u32[]{:S(2)}, u32[]{:S(2)}) collective-permute-start(bf16[1,512]{1,0:T(2,128)(2,1)S(1)} %get-tuple-element.14), channel_id=1, source_target_pairs={{4,0},{8,4},{12,8},{16,12},{20,16},{24,20},{28,24},{5,1},{9,5},{13... | collective-permute-start | bytes 3080 | tf_op jit(solution)/shard_map/ppermute | solution.py:15
Sparse Core Ops, SparseCore 0:
  36.1 21.5 all-gather.2
  59.3 22.5 all-gather.4
  93.1 31.1 reduce-scatter.2
  159.6 67.2 reduce-scatter.4
where the time goes:
time: 236 us; the launch traced here: 235 us
  waiting for transfers between devices  111 us (47%)
  blocking collectives  46.1 us (20%)
  matrix products  33.7 us (14%)
  between operations  14.1 us (6%)
  local copies, waits for them, and re-layouts  10.8 us (5%)
  starting transfers between devices  10.6 us (4%)
  other arithmetic  9.28 us (4%)
    reduce_scatter x1, waiting for transfers between devices, local(): lax.psum_scatter(lax.dot_general(full_h, mixed, (((0,), (0,)), ((), ())),...  47.1 us
    reduce_scatter x1, waiting for transfers between devices, local(): lax.psum_scatter(partial_value.astype(jnp.bfloat16), 'tp', scatter_dimens...  31.3 us
    all_to_all x1, blocking collectives, local(): lax.all_to_all(send_x, 'sp', split_axis=0, concat_axis=0, tiled=True)  21.7 us
    all_to_all x1, blocking collectives, local(): lax.all_to_all(send_dy, 'sp', split_axis=0, concat_axis=0, tiled=True)  17.6 us
    all_gather x1, waiting for transfers between devices, local(): lax.all_gather(part_dy, 'tp', axis=2, tiled=True)  16.8 us
    all_to_all x1, waiting for transfers between devices, local(): lax.all_to_all(summed.reshape(n_experts, capacity, local_cols), 'sp', spl...  14.3 us
    all_gather x1, blocking collectives, local(): full_h = lax.all_gather(grad_h, 'tp', axis=1, tiled=True)  6.72 us
    all_to_all x1, starting transfers between devices, local(): lax.all_to_all(summed.reshape(n_experts, capacity, local_cols), 'sp', spl...  5.51 us
  transfers between devices with their start and end apart: 7, of which 5 were waited for; matrix products, arithmetic and copies ran while one was open for 11% of the time, Pallas kernels for 0%

commit v1 on v0

--- a/solution.py
+++ b/solution.py
@@ -62,7 +62,7 @@
     )
     recv_x, recv_dy = (
         lax.all_gather(part_x, "tp", axis=2, tiled=True),
-        lax.all_gather(part_dy, "tp", axis=2, tiled=True),
+        jnp.concatenate(lax.all_gather(part_dy, "tp"), axis=2),
     )
     width = recv_x.shape[2]
     xin = recv_x.reshape(total, width)

time: 236 us -> 238 us (level)
  local copies, waits for them, and re-layouts: 10.8 us -> 16.5 us
  matrix products: 33.7 us -> 30.6 us
    reshape x0 -> x1, local copies, waits for them, and re-layouts: none -> 3.36 us  [local(): jnp.concatenate(lax.all_gather(part_dy, 'tp'), axis=2)]
    dot_general x1, matrix products: 5.37 us -> 2.13 us  [local(): dhid = jnp.dot(dyin, w_down.T, preferred_element_type=jnp.float32)]
where the time goes in v1:
time: 238 us; the launch traced here: 237 us
  waiting for transfers between devices  110 us (46%)
  blocking collectives  45.8 us (19%)
  matrix products  30.6 us (13%)
  local copies, waits for them, and re-layouts  16.5 us (7%)
  between operations  14.1 us (6%)
  starting transfers between devices  10.8 us (5%)
  other arithmetic  9.28 us (4%)
    reduce_scatter x1, waiting for transfers between devices, local(): lax.psum_scatter(lax.dot_general(full_h, mixed, (((0,), (0,)), ((), ())),...  46.9 us
    reduce_scatter x1, waiting for transfers between devices, local(): lax.psum_scatter(partial_value.astype(jnp.bfloat16), 'tp', scatter_dimens...  31.3 us
    all_to_all x1, blocking collectives, local(): lax.all_to_all(send_x, 'sp', split_axis=0, concat_axis=0, tiled=True)  21.7 us
    all_to_all x1, blocking collectives, local(): lax.all_to_all(send_dy, 'sp', split_axis=0, concat_axis=0, tiled=True)  17.6 us
    all_gather x1, waiting for transfers between devices, local(): lax.all_gather(part_dy, 'tp')  16.8 us
    all_to_all x1, waiting for transfers between devices, local(): lax.all_to_all(summed.reshape(n_experts, capacity, local_cols), 'sp', spl...  14 us
    all_gather x1, blocking collectives, local(): full_h = lax.all_gather(grad_h, 'tp', axis=1, tiled=True)  6.5 us
    all_to_all x1, starting transfers between devices, local(): lax.all_to_all(summed.reshape(n_experts, capacity, local_cols), 'sp', spl...  5.51 us
  transfers between devices with their start and end apart: 7, of which 5 were waited for; matrix products, arithmetic and copies ran while one was open for 11% of the time, Pallas kernels for 0%

profile of v1, /device:TPU:0, one launch (start us, length us, event | category | flops | bytes accessed | tf_op | source)
XLA Modules:
  0.0 237.2 jit_solution(6907593418958030995)
XLA Ops:
  7.2 0.9 copy.30
  10.2 1.0 broadcast_in_dim.8
  12.2 2.1 scatter_custom_fusion
  14.3 21.7 %all_to_all.15 = bf16[8,64,512]{2,1,0:T(8,128)(2,1)} all-to-all(bf16[8,64,512]{2,1,0:T(8,128)(2,1)S(1)} %bitcast.64), channel_id=1, replica_groups=mesh['sp'=8,'tp'=4] {'sp'}, dimensions={0} | all-to-all | bytes 1048576 | tf_op jit(solution)/shard_map/all_to_all | solution.py:60
  36.2 1.2 mul.110
  37.6 2.2 scatter_custom_fusion.1
  39.9 17.6 %all_to_all.16 = bf16[8,64,512]{2,1,0:T(8,128)(2,1)} all-to-all(bf16[8,64,512]{2,1,0:T(8,128)(2,1)S(1)} %bitcast.63), channel_id=1, replica_groups=mesh['sp'=8,'tp'=4] {'sp'}, dimensions={0} | all-to-all | bytes 1048576 | tf_op jit(solution)/shard_map/all_to_all | solution.py:61
  57.8 4.5 %fusion.5 = f32[512,704]{0,1:T(8,128)} fusion(bf16[512,2048]{1,0:T(8,128)(2,1)} %bitcast.73, bf16[1,2048,704]{1,2,0:T(8,128)(2,1)S(1)} %copy-done), kind=kOutput, calls=%fused_computation.13 | convolution fusion | flops 1476395008 | bytes 6422528 | tf_op jit(solution)/shard_map/dot_general | solution.py:73
  62.4 2.8 %fusion.8 = f32[512,704]{0,1:T(8,128)} fusion(bf16[512,2048]{1,0:T(8,128)(2,1)S(1)} %bitcast.75, bf16[1,2048,704]{1,2,0:T(8,128)(2,1)S(1)} %copy-done.14), kind=kOutput, calls=%fused_computation.16 | convolution fusion | flops 1476395008 | bytes 6422528 | tf_op jit(solution)/shard_map/dot_general | solution.py:74
  65.2 16.8 %all-gather.6.cloned.1.call-done = bf16[32,64,512]{2,1,0:T(8,128)(2,1)} async-done(((bf16[8,64,512]{2,1,0:T(8,128)(2,1)}), bf16[32,64,512]{2,1,0:T(8,128)(2,1)}) %all-gather.6.cloned.1.call-update) | async-done | bytes 2097168 | tf_op jit(solution)/shard_map/all_gather | solution.py:65
  81.9 3.4 %copy.33 = bf16[8,64,4,512]{3,2,1,0:T(4,128)(2,1)S(1)} copy(bf16[8,64,4,512]{3,1,0,2:T(8,128)(2,1)} %bitcast.62) | data formatting | bytes 4194304 | tf_op jit(solution)/shard_map/reshape | solution.py:65
  86.0 1.6 copy-done.13
  87.6 2.1 multiply_convert_fusion.1
  89.8 1.9 fusion.3
  92.1 3.3 %add_convert_fusion = bf16[512,2048]{1,0:T(8,128)(2,1)} fusion(f32[512,2048]{1,0:T(8,128)S(1)} %fusion.3, bf16[512,704]{0,1:T(8,128)(2,1)S(1)} %get-tuple-element.9, bf16[1,2048,704]{1,2,0:T(8,128)(2,1)S(1)} %copy-done.15), kind=kOutput, calls=%fused_computation.3 | convolution fusion | flops 1478492160 | bytes 9895936 | tf_op jit(solution)/shard_map/dot_general | solution.py:84
  95.5 31.3 %reduce-scatter.3.cloned.1.call-done = bf16[512,512]{1,0:T(8,128)(2,1)} async-done(((bf16[512,2048]{1,0:T(8,128)(2,1)}), bf16[512,512]{1,0:T(8,128)(2,1)}) %reduce-scatter.3.cloned.1.call-update) | async-done | bytes 524304 | tf_op jit(solution)/shard_map/reduce_scatter | solution.py:88
  126.8 5.5 %all-to-all-start.2 = ((bf16[8,64,512]{2,1,0:T(8,128)(2,1)}), bf16[8,64,512]{2,1,0:T(8,128)(2,1)S(1)}, u32[]{:S(2)}, u32[]{:S(2)}) async-start(bf16[8,64,512]{2,1,0:T(8,128)(2,1)} %bitcast.65), calls=%async_computation.3 | async-start | bytes 1048576 | tf_op jit(solution)/shard_map/all_to_all | solution.py:91
  132.6 14.0 %all-to-all-done.2 = bf16[8,64,512]{2,1,0:T(8,128)(2,1)S(1)} async-done(((bf16[8,64,512]{2,1,0:T(8,128)(2,1)}), bf16[8,64,512]{2,1,0:T(8,128)(2,1)S(1)}, u32[]{:S(2)}, u32[]{:S(2)}) %all-to-all-start.2) | async-done | bytes 524320 | tf_op jit(solution)/shard_map/all_to_all | solution.py:91
  146.6 1.9 gather_fusion
  148.5 1.3 reshape.99
  149.8 1.3 reduce_sum.22
  151.1 1.0 add_convert_fusion.1
  152.1 6.5 %all_gather.15 = bf16[128,2048]{1,0:T(8,128)(2,1)S(1)} all-gather(bf16[128,512]{1,0:T(8,128)(2,1)S(1)} %add_convert_fusion.1), channel_id=1, replica_groups=mesh['sp'=8,'tp'=4] {'tp'}, dimensions={1}, use_global_device_ids=true | all-gather | bytes 655360 | tf_op jit(solution)/shard_map/all_gather | solution.py:101
  158.6 3.0 %convolution_convert_fusion.3 = bf16[2048,512]{1,0:T(8,128)(2,1)} fusion(bf16[128,2048]{1,0:T(8,128)(2,1)S(1)} %all_gather.15, bf16[128,512]{1,0:T(8,128)(2,1)S(1)} %copy-done.6, bf16[128,512]{1,0:T(8,128)(2,1)} %param.22), kind=kOutput, calls=%fused_computation.7 | convolution fusion | flops 269746176 | bytes 2883584 | tf_op jit(solution)/shard_map/dot_general | solution.py:111
  161.7 5.2 %fusion.2 = bf16[1,2048,704]{1,2,0:T(8,128)(2,1)} fusion(bf16[512,704]{0,1:T(8,128)(2,1)} %copy-done.18, bf16[512,2048]{1,0:T(8,128)(2,1)} %bitcast.74), kind=kOutput, calls=%fused_computation.10 | convolution fusion | flops 1477836800 | bytes 5701632 | tf_op jit(solution)/shard_map/dot_general | solution.py:83
  166.9 3.3 %fusion = bf16[1,704,2048]{2,1,0:T(8,128)(2,1)} fusion(bf16[512,2048]{1,0:T(8,128)(2,1)S(1)} %bitcast.61, f32[512,704]{0,1:T(8,128)S(1)} %copy-done.22, f32[512,704]{0,1:T(8,128)S(1)} %copy-done.20), kind=kOutput, calls=%fused_computation.8 | convolution fusion | flops 1479999488 | bytes 7864320 | tf_op jit(solution)/shard_map/dot_general | solution.py:78
  170.2 1.2 fusion.13
  171.4 3.4 %collective-permute-start = (bf16[1,512]{1,0:T(2,128)(2,1)S(1)}, bf16[1,512]{1,0:T(2,128)(2,1)S(1)}, u32[]{:S(2)}, u32[]{:S(2)}) collective-permute-start(bf16[1,512]{1,0:T(2,128)(2,1)S(1)} %get-tuple-element.13), channel_id=1, source_target_pairs={{0,4},{4,8},{8,12},{12,16},{16,20},{20,24},{24,28},{1,5},{5,9},{9,... | collective-permute-start | bytes 3080 | tf_op jit(solution)/shard_map/ppermute | solution.py:12
  174.8 1.4 collective-permute-start.1
  176.2 3.3 %fusion.1 = bf16[1,2048,704]{1,2,0:T(8,128)(2,1)} fusion(bf16[512,704]{0,1:T(8,128)(2,1)S(1)} %copy-done.5, bf16[512,2048]{1,0:T(8,128)(2,1)S(1)} %bitcast.76), kind=kOutput, calls=%fused_computation.9 | convolution fusion | flops 1477836800 | bytes 5701632 | tf_op jit(solution)/shard_map/dot_general | solution.py:82
  181.9 46.9 %reduce-scatter.5.cloned.1.call-done = bf16[256,512]{1,0:T(8,128)(2,1)} async-done(((bf16[2048,512]{1,0:T(8,128)(2,1)}), bf16[256,512]{1,0:T(8,128)(2,1)}) %reduce-scatter.5.cloned.1.call-update) | async-done | bytes 262160 | tf_op jit(solution)/shard_map/reduce_scatter | solution.py:110
  228.8 1.8 convert_element_type.103
  (79 shorter events, 7.5 us)
Async XLA Ops:
  7.2 50.6 %copy-start = (bf16[1,2048,704]{1,2,0:T(8,128)(2,1)S(1)}, bf16[1,2048,704]{1,2,0:T(8,128)(2,1)}, u32[]{:S(2)}) copy-start(bf16[1,2048,704]{1,2,0:T(8,128)(2,1)} %param.17) | copy-start | bytes 8650756
  7.2 28.9 %copy-start.8 = (bf16[128,512]{1,0:T(8,128)(2,1)S(1)}, bf16[128,512]{1,0:T(8,128)(2,1)}, u32[]{:S(2)}) copy-start(bf16[128,512]{1,0:T(8,128)(2,1)} %param.13) | copy-start | bytes 393220
  7.2 50.6 %all-gather.4.cloned.1.call-start = ((), (), s32[]{:S(2)}) async-start(), calls=%async_computation.5 | async-start | bytes 2621440 | tf_op jit(solution)/shard_map/all_gather | solution.py:64
  11.3 26.1 %copy-start.12 = (f32[128,2]{0,1:T(2,128)S(1)}, f32[128,2]{0,1:T(2,128)}, u32[]{:S(2)}) copy-start(f32[128,2]{0,1:T(2,128)} %param.15) | copy-start | bytes 3076
  36.0 45.9 %all-gather.6.cloned.1.call-start = ((), (), s32[]{:S(2)}) async-start(), calls=%async_computation.8 | async-start | bytes 2621440 | tf_op jit(solution)/shard_map/all_gather | solution.py:65
  57.5 69.3 %reduce-scatter.3.cloned.1.call-start = ((), (), s32[]{:S(2)}) async-start(), calls=%async_computation.6 | async-start | bytes 2621440 | tf_op jit(solution)/shard_map/reduce_scatter | solution.py:88
  57.8 4.6 %copy-start.14 = (bf16[1,2048,704]{1,2,0:T(8,128)(2,1)S(1)}, bf16[1,2048,704]{1,2,0:T(8,128)(2,1)}, u32[]{:S(2)}) copy-start(bf16[1,2048,704]{1,2,0:T(8,128)(2,1)} %param.18) | copy-start | bytes 8650756
  57.8 4.5 %copy-start.16 = (bf16[8,64,2048]{2,1,0:T(8,128)(2,1)S(1)}, bf16[8,64,2048]{2,1,0:T(8,128)(2,1)}, u32[]{:S(2)}) copy-start(bf16[8,64,2048]{2,1,0:T(8,128)(2,1)} %all-gather.4.cloned.1.call-done) | copy-start | bytes 6291460
  81.9 4.0 %copy-start.19 = (f32[512,704]{0,1:T(8,128)S(1)}, f32[512,704]{0,1:T(8,128)}, u32[]{:S(2)}) copy-start(f32[512,704]{0,1:T(8,128)} %fusion.5) | copy-start | bytes 4325380
  81.9 4.0 %copy-start.21 = (f32[512,704]{0,1:T(8,128)S(1)}, f32[512,704]{0,1:T(8,128)}, u32[]{:S(2)}) copy-start(f32[512,704]{0,1:T(8,128)} %fusion.8) | copy-start | bytes 4325380
  85.3 2.3 copy-start.13
  85.9 3.8 %copy-start.2 = (bf16[64,8,4,512]{3,1,2,0:T(8,128)(2,1)}, bf16[64,8,4,512]{3,1,2,0:T(8,128)(2,1)S(1)}, u32[]{:S(2)}) copy-start(bf16[64,8,4,512]{3,1,2,0:T(8,128)(2,1)S(1)} %copy.34) | copy-start | bytes 6291460
  89.8 1.9 copy-start.4
  89.8 1.9 copy-start.18
  89.8 2.3 copy-start.15
  126.8 19.8 %all-to-all-start.2 = ((bf16[8,64,512]{2,1,0:T(8,128)(2,1)}), bf16[8,64,512]{2,1,0:T(8,128)(2,1)S(1)}, u32[]{:S(2)}, u32[]{:S(2)}) async-start(bf16[8,64,512]{2,1,0:T(8,128)(2,1)} %bitcast.65), calls=%async_computation.3 | async-start | bytes 1048576 | tf_op jit(solution)/shard_map/all_to_all | solution.py:91
  132.3 96.5 %reduce-scatter.5.cloned.1.call-start = ((), (), s32[]{:S(2)}) async-start(), calls=%async_computation.7 | async-start | bytes 2359296 | tf_op jit(solution)/shard_map/reduce_scatter | solution.py:110
  146.6 12.0 %copy-start.6 = (bf16[128,512]{1,0:T(8,128)(2,1)S(1)}, bf16[128,512]{1,0:T(8,128)(2,1)}, u32[]{:S(2)}) copy-start(bf16[128,512]{1,0:T(8,128)(2,1)} %param.21) | copy-start | bytes 393220
  158.6 3.0 %copy-start.11 = (f32[3,512]{1,0:T(4,128)S(1)}, f32[3,512]{1,0:T(4,128)}, u32[]{:S(2)}) copy-start(f32[3,512]{1,0:T(4,128)} %param.25) | copy-start | bytes 18436
  161.7 5.2 %copy-start.3 = (bf16[64,8,4,512]{3,1,2,0:T(8,128)(2,1)S(1)}, bf16[64,8,4,512]{3,1,2,0:T(8,128)(2,1)}, u32[]{:S(2)}) copy-start(bf16[64,8,4,512]{3,1,2,0:T(8,128)(2,1)} %copy-done.2) | copy-start | bytes 6291460
  161.7 5.2 %copy-start.20 = (f32[512,704]{0,1:T(8,128)S(1)}, f32[512,704]{0,1:T(8,128)}, u32[]{:S(2)}) copy-start(f32[512,704]{0,1:T(8,128)} %fusion.5) | copy-start | bytes 4325380
  161.7 5.2 %copy-start.22 = (f32[512,704]{0,1:T(8,128)S(1)}, f32[512,704]{0,1:T(8,128)}, u32[]{:S(2)}) copy-start(f32[512,704]{0,1:T(8,128)} %fusion.8) | copy-start | bytes 4325380
  166.9 3.3 %copy-start.1 = (bf16[2048,512]{1,0:T(8,128)(2,1)S(1)}, bf16[2048,512]{1,0:T(8,128)(2,1)}, u32[]{:S(2)}) copy-start(bf16[2048,512]{1,0:T(8,128)(2,1)} %param.20) | copy-start | bytes 6291460
  166.9 3.3 %copy-start.7 = (bf16[128,512]{1,0:T(8,128)(2,1)S(1)}, bf16[128,512]{1,0:T(8,128)(2,1)}, u32[]{:S(2)}) copy-start(bf16[128,512]{1,0:T(8,128)(2,1)} %param.22) | copy-start | bytes 393220
  170.2 6.0 %copy-start.5 = (bf16[512,704]{0,1:T(8,128)(2,1)S(1)}, bf16[512,704]{0,1:T(8,128)(2,1)}, u32[]{:S(2)}) copy-start(bf16[512,704]{0,1:T(8,128)(2,1)} %copy-done.4) | copy-start | bytes 2162692
  170.2 6.0 %copy-start.17 = (bf16[8,64,2048]{2,1,0:T(8,128)(2,1)S(1)}, bf16[8,64,2048]{2,1,0:T(8,128)(2,1)}, u32[]{:S(2)}) copy-start(bf16[8,64,2048]{2,1,0:T(8,128)(2,1)} %all-gather.4.cloned.1.call-done) | copy-start | bytes 6291460
  171.4 8.1 %collective-permute-start = (bf16[1,512]{1,0:T(2,128)(2,1)S(1)}, bf16[1,512]{1,0:T(2,128)(2,1)S(1)}, u32[]{:S(2)}, u32[]{:S(2)}) collective-permute-start(bf16[1,512]{1,0:T(2,128)(2,1)S(1)} %get-tuple-element.13), channel_id=1, source_target_pairs={{0,4},{4,8},{8,12},{12,16},{16,20},{20,24},{24,28},{1,5},{5,9},{9,... | collective-permute-start | bytes 3080 | tf_op jit(solution)/shard_map/ppermute | solution.py:12
  174.8 5.7 %copy-start.9 = (bf16[128,512]{1,0:T(8,128)(2,1)S(1)}, bf16[128,512]{1,0:T(8,128)(2,1)}, u32[]{:S(2)}) copy-start(bf16[128,512]{1,0:T(8,128)(2,1)} %param.23) | copy-start | bytes 393220
  174.8 6.4 %copy-start.10 = (bf16[128,512]{1,0:T(8,128)(2,1)S(1)}, bf16[128,512]{1,0:T(8,128)(2,1)}, u32[]{:S(2)}) copy-start(bf16[128,512]{1,0:T(8,128)(2,1)} %param.24) | copy-start | bytes 393220
  174.8 5.6 %collective-permute-start.1 = (bf16[1,512]{1,0:T(2,128)(2,1)S(1)}, bf16[1,512]{1,0:T(2,128)(2,1)S(1)}, u32[]{:S(2)}, u32[]{:S(2)}) collective-permute-start(bf16[1,512]{1,0:T(2,128)(2,1)S(1)} %get-tuple-element.14), channel_id=1, source_target_pairs={{4,0},{8,4},{12,8},{16,12},{20,16},{24,20},{28,24},{5,1},{9,5},{13... | collective-permute-start | bytes 3080 | tf_op jit(solution)/shard_map/ppermute | solution.py:15
Sparse Core Ops, SparseCore 0:
  36.1 21.5 all-gather.3
  59.3 22.5 all-gather.5
  95.6 31.1 reduce-scatter.2
  161.8 67.0 reduce-scatter.4
